TPU v7x, 32 devices: a whole 2x2x4 slice. The times are simulated.
32 devices in a mesh: sp: 8 (over z, y), tp: 4 (over x, core).
Axes of the slice: x: 2, y: 2, z: 4, core: 2. Of those that a mesh axis runs over, the one named last changes fastest.
Arguments:
- mixer_out: bfloat16 [1024, 2048], P('sp'), may hold values from -6 to 6
- conv_out: bfloat16 [1024, 2048], P('sp', 'tp'), may hold values from -350 to 350
- out_cot: bfloat16 [1024, 2048], P('sp'), may hold values from -6 to 6
- routes: int32 [1024, 2], P('sp'), may hold values from 0 to 7, all different within a row; in each aligned block of 128 rows (0 to 127, 128 to 255, ...) at most 64 rows name the same one
- route_weight: float32 [1024, 2], P('sp'), may hold values from 0.3 to 2.5
- gate_weight: bfloat16 [8, 2048, 1024], P('sp', None, 'tp'), may hold values from -0.125 to 0.125
- up_weight: bfloat16 [8, 2048, 1024], P('sp', None, 'tp'), may hold values from -0.125 to 0.125
- down_weight: bfloat16 [8, 1024, 2048], P('sp', 'tp'), may hold values from -0.1875 to 0.1875
- out_weight: bfloat16 [2048, 2048], P('tp'), may hold values from -0.125 to 0.125
- norm_gain: float32 [2048], P('tp'), may hold values from 0.1 to 1.9
- conv_taps: float32 [31, 2048], P(None, 'tp'), may hold values from -1 to 1
Outputs:
- gate_grad: bfloat16 [8, 2048, 1024], P('sp', None, 'tp')
- up_grad: bfloat16 [8, 2048, 1024], P('sp', None, 'tp')
- down_grad: bfloat16 [8, 1024, 2048], P('sp', 'tp')
- proj_grad: float32 [2048, 2048], P('sp', 'tp')
- gated_grad: float32 [1024, 2048], P('sp', 'tp')
Inputs may be any that keep to these rules, and one draw needn't show every extreme that they name: `routes`: each row names 2 different experts. Among the rows of one device no expert is named by more than 64 rows, and in every draw some expert is named by exactly 64 rows of some device.
All inputs are finite; a program needn't handle non-finite values.
Results may differ from a plain program's by a relative error of at most 0.0095.
Values may be sent and summed in bfloat16 or wider, within the bound.
A program may use at most 64 MiB of HBM per device.

v0:
```python
import jax
import jax.numpy as jnp
from jax import lax
from jax.sharding import PartitionSpec as P

norm_epsilon = 1e-05


def shifted(block, axis, distance):
    devices = range(lax.axis_size(axis))
    route = [(i - distance, i) for i in devices if i - distance in devices]
    return lax.ppermute(block, axis, route)


def expert_backward(x_rows, cot_rows, w_gate, w_up, w_down):
    pre_gate = jnp.dot(x_rows, w_gate, preferred_element_type=jnp.float32)
    pre_up = jnp.dot(x_rows, w_up, preferred_element_type=jnp.float32)
    sig_gate = jax.nn.sigmoid(pre_gate)
    activation = (pre_gate * sig_gate * pre_up).astype(jnp.bfloat16)
    down_g = lax.dot_general(
        activation, cot_rows, (((0,), (0,)), ((), ())), preferred_element_type=jnp.float32
    ).astype(jnp.bfloat16)
    act_grad = lax.dot_general(
        cot_rows, w_down, (((1,), (1,)), ((), ())), preferred_element_type=jnp.float32
    )
    gate_pre_grad = (act_grad * pre_up * sig_gate * (1.0 + pre_gate * (1.0 - sig_gate))).astype(
        jnp.bfloat16
    )
    up_pre_grad = (act_grad * pre_gate * sig_gate).astype(jnp.bfloat16)
    gate_g = lax.dot_general(
        x_rows, gate_pre_grad, (((0,), (0,)), ((), ())), preferred_element_type=jnp.float32
    ).astype(jnp.bfloat16)
    up_g = lax.dot_general(
        x_rows, up_pre_grad, (((0,), (0,)), ((), ())), preferred_element_type=jnp.float32
    ).astype(jnp.bfloat16)
    partial_value = lax.dot_general(
        gate_pre_grad, w_gate, (((1,), (1,)), ((), ())), preferred_element_type=jnp.float32
    )
    partial_value = partial_value + lax.dot_general(
        up_pre_grad, w_up, (((1,), (1,)), ((), ())), preferred_element_type=jnp.float32
    )
    rounded = lax.optimization_barrier(partial_value.astype(jnp.bfloat16))
    return (gate_g, up_g, down_g, rounded.astype(jnp.float32))


def on_device(
    mixer_out,
    conv_out,
    out_cot,
    routes,
    route_weight,
    gate_weight,
    up_weight,
    down_weight,
    out_weight,
    norm_gain,
    conv_taps,
):
    tokens_here, model_width = out_cot.shape
    route_count = routes.shape[1]
    experts = lax.axis_size("sp")
    capacity = 2 * tokens_here * route_count // experts
    quarter = conv_out.shape[1]
    first_col = lax.axis_index("tp") * quarter
    flat_routes = routes.reshape(-1)
    one_hot = (flat_routes[:, None] == jnp.arange(experts, dtype=jnp.int32)[None, :]).astype(
        jnp.int32
    )
    within = jnp.sum((jnp.cumsum(one_hot, axis=0) - one_hot) * one_hot, axis=1)
    slot_index = flat_routes * capacity + within
    row_cot = (route_weight[:, :, None] * out_cot[:, None, :].astype(jnp.float32)).astype(
        jnp.bfloat16
    )
    row_cot = row_cot.reshape(tokens_here * route_count, model_width)
    rows_input = jnp.repeat(mixer_out, route_count, axis=0)
    w_gate = gate_weight[0]
    w_up = up_weight[0]
    w_down = down_weight[0]
    rows_part = lax.dynamic_slice_in_dim(rows_input, first_col, quarter, 1)
    cot_part = lax.dynamic_slice_in_dim(row_cot, first_col, quarter, 1)
    send_rows = jnp.zeros((experts * capacity, quarter), jnp.bfloat16).at[slot_index].set(rows_part)
    send_cot = jnp.zeros((experts * capacity, quarter), jnp.bfloat16).at[slot_index].set(cot_part)
    rows_slice, cot_slice = (
        lax.all_to_all(send_rows, "sp", split_axis=0, concat_axis=0, tiled=True),
        lax.all_to_all(send_cot, "sp", split_axis=0, concat_axis=0, tiled=True),
    )
    x_rows, cot_rows = (
        lax.all_gather(rows_slice, "tp", axis=1, tiled=True),
        lax.all_gather(cot_slice, "tp", axis=1, tiled=True),
    )
    gate_g, up_g, down_g, partial_value = expert_backward(x_rows, cot_rows, w_gate, w_up, w_down)
    back_slice = lax.psum_scatter(
        partial_value.astype(jnp.bfloat16), "tp", scatter_dimension=1, tiled=True
    )
    returned = lax.all_to_all(back_slice, "sp", split_axis=0, concat_axis=0, tiled=True)
    picked = returned[slot_index].astype(jnp.float32).reshape(tokens_here, route_count, quarter)
    own_cot = lax.dynamic_slice_in_dim(out_cot, first_col, quarter, 1).astype(jnp.float32)
    mix_part = (own_cot + jnp.sum(picked, axis=1)).astype(jnp.bfloat16)
    mix_grad = lax.all_gather(mix_part, "tp", axis=1, tiled=True)
    conv_vals = conv_out.astype(jnp.float32)
    power_sum = lax.psum(jnp.sum(conv_vals * conv_vals, axis=1), "tp")
    inv_rms = lax.rsqrt(power_sum / model_width + norm_epsilon)[:, None]
    normed = conv_vals * inv_rms * norm_gain[None, :]
    sig_norm = jax.nn.sigmoid(normed)
    activated = (normed * sig_norm).astype(jnp.bfloat16)
    proj_grad = lax.psum_scatter(
        lax.dot_general(
            mix_grad, activated, (((0,), (0,)), ((), ())), preferred_element_type=jnp.float32
        ),
        "sp",
        scatter_dimension=0,
        tiled=True,
    )
    norm_in_grad = lax.dot_general(
        mix_grad, out_weight, (((1,), (1,)), ((), ())), preferred_element_type=jnp.float32
    )
    scaled = norm_in_grad * sig_norm * (1.0 + normed * (1.0 - sig_norm)) * norm_gain[None, :]
    dot_sum = lax.psum(jnp.sum(conv_vals * scaled, axis=1), "tp")
    conv_grad = inv_rms * scaled - conv_vals * inv_rms**3 * (dot_sum / model_width)[:, None]
    reach = conv_taps.shape[0] - 1
    following = shifted(conv_grad[:reach].astype(jnp.bfloat16), "sp", -1).astype(jnp.float32)
    extended = jnp.concatenate([conv_grad, following], axis=0)
    gated_grad = jnp.zeros((tokens_here, quarter), jnp.float32)
    for tap_index in range(reach + 1):
        gated_grad = (
            gated_grad
            + conv_taps[tap_index][None, :] * extended[tap_index : tap_index + tokens_here]
        )
    return (gate_g[None], up_g[None], down_g[None], proj_grad, gated_grad)


def solution(mesh):
    placed = (
        P("sp", None),
        P("sp", "tp"),
        P("sp", None),
        P("sp", None),
        P("sp", None),
        P("sp", None, "tp"),
        P("sp", None, "tp"),
        P("sp", "tp", None),
        P("tp", None),
        P("tp"),
        P(None, "tp"),
    )
    return jax.shard_map(
        on_device,
        mesh=mesh,
        in_specs=placed,
        out_specs=(
            P("sp", None, "tp"),
            P("sp", None, "tp"),
            P("sp", "tp", None),
            P("sp", "tp"),
            P("sp", "tp"),
        ),
        check_vma=False,
    )
```

profile of v0, /device:TPU:0, one launch (start us, length us, event | category | flops | bytes accessed | tf_op | source)
XLA Modules:
  0.0 249.0 jit_solution(12944334722822858562)
XLA Ops:
  7.2 0.8 broadcast_multiply_fusion
  10.2 1.7 broadcast_in_dim.8
  11.9 1.2 reshape.83
  13.2 2.1 scatter_custom_fusion
  15.3 21.7 %all_to_all.36 = bf16[8,64,512]{2,1,0:T(8,128)(2,1)} all-to-all(bf16[8,64,512]{2,1,0:T(8,128)(2,1)S(1)} %bitcast.85), channel_id=1, replica_groups=mesh['sp'=8,'tp'=4] {'sp'}, dimensions={0} | all-to-all | bytes 1048576 | tf_op jit(solution)/shard_map/all_to_all | solution.py:84
  37.1 2.4 mul.443
  39.5 3.7 %mul.444 = f32[256,2048]{1,0:T(8,128)} reshape(f32[128,2,2048]{2,1,0:T(2,128)} %mul.443) | data formatting | bytes 4194304 | tf_op jit(solution)/shard_map/mul | solution.py:71
  43.4 2.4 scatter_custom_fusion.1
  45.8 17.5 %all_to_all.37 = bf16[8,64,512]{2,1,0:T(8,128)(2,1)} all-to-all(bf16[8,64,512]{2,1,0:T(8,128)(2,1)S(1)} %bitcast.84), channel_id=1, replica_groups=mesh['sp'=8,'tp'=4] {'sp'}, dimensions={0} | all-to-all | bytes 1048576 | tf_op jit(solution)/shard_map/all_to_all | solution.py:85
  63.4 3.5 %fusion.7 = f32[512,256]{1,0:T(8,128)} fusion(bf16[512,2048]{1,0:T(8,128)(2,1)} %all-gather.3.cloned.1.call-done, bf16[1,2048,256]{2,1,0:T(8,128)(2,1)} %param.16), kind=kOutput, calls=%fused_computation.44 | convolution fusion | flops 536870912 | bytes 3670016 | tf_op jit(solution)/shard_map/dot_general | solution.py:16
  66.9 1.5 fusion.10
  68.4 16.7 %all-gather.5.cloned.1.call-done = bf16[512,2048]{1,0:T(8,128)(2,1)} async-done(((bf16[512,512]{1,0:T(8,128)(2,1)}), bf16[512,2048]{1,0:T(8,128)(2,1)}) %all-gather.5.cloned.1.call-update) | async-done | bytes 2097168 | tf_op jit(solution)/shard_map/all_gather | solution.py:89
  85.1 3.0 %multiply_convert_fusion.1 = (bf16[512,256]{1,0:T(8,128)(2,1)S(1)}, bf16[512,256]{1,0:T(8,128)(2,1)S(1)}) fusion(f32[512,256]{1,0:T(8,128)} %fusion.7, f32[512,256]{1,0:T(8,128)} %fusion.10, bf16[512,2048]{1,0:T(8,128)(2,1)} %all-gather.5.cloned.1.call-done, bf16[1,256,2048]{2,1,0:T(8,128)(2,1)} %param.18), kind=kOutput, calls=%fused_computation.83 | convolution fusion | flops 538574848 | bytes 4718592 | tf_op jit(solution)/shard_map/dot_general | solution.py:23
  89.4 2.1 add_convert_fusion
  91.5 31.3 %reduce-scatter.3.cloned.1.call-done = bf16[512,512]{1,0:T(8,128)(2,1)} async-done(((bf16[512,2048]{1,0:T(8,128)(2,1)}), bf16[512,512]{1,0:T(8,128)(2,1)}) %reduce-scatter.3.cloned.1.call-update) | async-done | bytes 524304 | tf_op jit(solution)/shard_map/reduce_scatter | solution.py:92
  122.8 5.5 %all-to-all-start.2 = ((bf16[8,64,512]{2,1,0:T(8,128)(2,1)}), bf16[8,64,512]{2,1,0:T(8,128)(2,1)S(1)}, u32[]{:S(2)}, u32[]{:S(2)}) async-start(bf16[8,64,512]{2,1,0:T(8,128)(2,1)} %bitcast.86), calls=%async_computation.3 | async-start | bytes 1048576 | tf_op jit(solution)/shard_map/all_to_all | solution.py:95
  128.5 6.0 %psum.14 = f32[128]{0:T(128)S(1)} all-reduce(f32[128]{0:T(128)S(1)} %fusion.15), channel_id=1, replica_groups=mesh['sp'=8,'tp'=4] {'tp'}, use_global_device_ids=true, to_apply=%region_8.9 | all-reduce | flops 128 | bytes 1024 | tf_op jit(solution)/shard_map/psum | solution.py:101
  134.5 8.2 %all-to-all-done.2 = bf16[8,64,512]{2,1,0:T(8,128)(2,1)S(1)} async-done(((bf16[8,64,512]{2,1,0:T(8,128)(2,1)}), bf16[8,64,512]{2,1,0:T(8,128)(2,1)S(1)}, u32[]{:S(2)}, u32[]{:S(2)}) %all-to-all-start.2) | async-done | bytes 524320 | tf_op jit(solution)/shard_map/all_to_all | solution.py:95
  142.7 1.2 gather_fusion
  144.8 0.9 add_convert_fusion.1
  145.7 6.7 %all_gather.11 = bf16[128,2048]{1,0:T(8,128)(2,1)S(1)} all-gather(bf16[128,512]{1,0:T(8,128)(2,1)S(1)} %add_convert_fusion.1), channel_id=1, replica_groups=mesh['sp'=8,'tp'=4] {'tp'}, dimensions={1}, use_global_device_ids=true | all-gather | bytes 655360 | tf_op jit(solution)/shard_map/all_gather | solution.py:99
  152.4 2.8 %fusion.125 = f32[2048,512]{1,0:T(8,128)} fusion(bf16[128,2048]{1,0:T(8,128)(2,1)S(1)} %all_gather.11, bf16[128,512]{1,0:T(8,128)(2,1)S(1)} %copy-done.2, f32[512]{0:T(512)S(1)} %copy-done.12, f32[128]{0:T(128)S(1)} %get-tuple-element.39), kind=kOutput, calls=%fused_computation.201 | convolution fusion | flops 268959744 | bytes 4852224 | tf_op jit(solution)/shard_map/dot_general | solution.py:107
  155.2 0.8 copy-done.11
  156.2 3.5 %fusion = bf16[1,2048,256]{2,1,0:T(8,128)(2,1)} fusion(bf16[512,2048]{1,0:T(8,128)(2,1)} %all-gather.3.cloned.1.call-done, bf16[512,256]{1,0:T(8,128)(2,1)S(1)} %get-tuple-element.6), kind=kOutput, calls=%fused_computation.36 | convolution fusion | flops 537395200 | bytes 3407872 | tf_op jit(solution)/shard_map/dot_general | solution.py:30
  159.6 1.8 fusion.2
  161.4 0.9 fusion.27
  162.3 7.2 %psum.15 = f32[128]{0:T(128)S(1)} all-reduce(f32[128]{0:T(128)S(1)} %get-tuple-element.40), channel_id=1, replica_groups=mesh['sp'=8,'tp'=4] {'tp'}, use_global_device_ids=true, to_apply=%region_11.12 | all-reduce | flops 128 | bytes 1024 | tf_op jit(solution)/shard_map/psum | solution.py:118
  169.7 1.3 collective-permute-start
  171.0 3.3 %fusion.1 = bf16[1,2048,256]{2,1,0:T(8,128)(2,1)} fusion(bf16[512,2048]{1,0:T(8,128)(2,1)} %all-gather.3.cloned.1.call-done, bf16[512,256]{1,0:T(8,128)(2,1)S(1)} %copy-done.10), kind=kOutput, calls=%fused_computation.37 | convolution fusion | flops 537395200 | bytes 3407872 | tf_op jit(solution)/shard_map/dot_general | solution.py:33
  174.4 1.1 collective-permute-done
  175.5 1.4 fusion.33
  176.9 65.6 %reduce-scatter.5.cloned.1.call-done = f32[256,512]{1,0:T(8,128)} async-done(((f32[2048,512]{1,0:T(8,128)}), f32[256,512]{1,0:T(8,128)}) %reduce-scatter.5.cloned.1.call-update) | async-done | bytes 524304 | tf_op jit(solution)/shard_map/reduce_scatter | solution.py:106
  (64 shorter events, 5.4 us)
Async XLA Ops:
  7.2 154.2 %copy-start = (bf16[512,2048]{1,0:T(8,128)(2,1)S(1)}, bf16[512,2048]{1,0:T(8,128)(2,1)}, u32[]{:S(2)}) copy-start(bf16[512,2048]{1,0:T(8,128)(2,1)} %param.19) | copy-start | bytes 6291460
  7.2 56.2 %all-gather.3.cloned.1.call-start = ((), (), s32[]{:S(2)}) async-start(), calls=%async_computation.5 | async-start | bytes 2621440 | tf_op jit(solution)/shard_map/all_gather | solution.py:88
  13.1 24.0 %copy-start.6 = (bf16[128,2048]{1,0:T(8,128)(2,1)S(1)}, bf16[128,2048]{1,0:T(8,128)(2,1)}, u32[]{:S(2)}) copy-start(bf16[128,2048]{1,0:T(8,128)(2,1)} %param.13) | copy-start | bytes 1572868
  37.1 48.0 %all-gather.5.cloned.1.call-start = ((), (), s32[]{:S(2)}) async-start(), calls=%async_computation.6 | async-start | bytes 2621440 | tf_op jit(solution)/shard_map/all_gather | solution.py:89
  39.5 3.7 %copy-start.13 = (f32[128,2]{0,1:T(2,128)S(1)}, f32[128,2]{0,1:T(2,128)}, u32[]{:S(2)}) copy-start(f32[128,2]{0,1:T(2,128)} %param.15) | copy-start | bytes 3076
  63.3 3.6 %copy-start.4 = (bf16[1,2048,256]{2,1,0:T(8,128)(2,1)S(1)}, bf16[1,2048,256]{2,1,0:T(8,128)(2,1)}, u32[]{:S(2)}) copy-start(bf16[1,2048,256]{2,1,0:T(8,128)(2,1)} %param.17) | copy-start | bytes 3145732
  63.3 59.5 %reduce-scatter.3.cloned.1.call-start = ((), (), s32[]{:S(2)}) async-start(), calls=%async_computation.7 | async-start | bytes 2621440 | tf_op jit(solution)/shard_map/reduce_scatter | solution.py:92
  63.4 3.5 %copy-start.14 = (bf16[512,2048]{1,0:T(8,128)(2,1)S(1)}, bf16[512,2048]{1,0:T(8,128)(2,1)}, u32[]{:S(2)}) copy-start(bf16[512,2048]{1,0:T(8,128)(2,1)} %all-gather.3.cloned.1.call-done) | copy-start | bytes 6291460
  68.4 19.6 %copy-start.3 = (bf16[1,2048,256]{2,1,0:T(8,128)(2,1)S(1)}, bf16[1,2048,256]{2,1,0:T(8,128)(2,1)}, u32[]{:S(2)}) copy-start(bf16[1,2048,256]{2,1,0:T(8,128)(2,1)} %param.16) | copy-start | bytes 3145732
  88.1 0.8 copy-start.9
  88.1 1.3 copy-start.5
  91.5 36.9 %copy-start.2 = (bf16[128,512]{1,0:T(8,128)(2,1)S(1)}, bf16[128,512]{1,0:T(8,128)(2,1)}, u32[]{:S(2)}) copy-start(bf16[128,512]{1,0:T(8,128)(2,1)} %param.12) | copy-start | bytes 393220
  122.8 19.8 %all-to-all-start.2 = ((bf16[8,64,512]{2,1,0:T(8,128)(2,1)}), bf16[8,64,512]{2,1,0:T(8,128)(2,1)S(1)}, u32[]{:S(2)}, u32[]{:S(2)}) async-start(bf16[8,64,512]{2,1,0:T(8,128)(2,1)} %bitcast.86), calls=%async_computation.3 | async-start | bytes 1048576 | tf_op jit(solution)/shard_map/all_to_all | solution.py:95
  128.4 114.1 %reduce-scatter.5.cloned.1.call-start = ((), (), s32[]{:S(2)}) async-start(), calls=%async_computation.8 | async-start | bytes 4718592 | tf_op jit(solution)/shard_map/reduce_scatter | solution.py:106
  142.7 9.7 %copy-start.12 = (f32[512]{0:T(512)S(1)}, f32[512]{0:T(512)}, u32[]{:S(2)}) copy-start(f32[512]{0:T(512)} %param.20) | copy-start | bytes 6148
  155.2 0.8 copy-start.11
  156.1 3.5 %copy-start.1 = (bf16[512,2048]{1,0:T(8,128)(2,1)S(1)}, bf16[512,2048]{1,0:T(8,128)(2,1)}, u32[]{:S(2)}) copy-start(bf16[512,2048]{1,0:T(8,128)(2,1)} %all-gather.5.cloned.1.call-done) | copy-start | bytes 6291460
  156.1 3.5 %copy-start.7 = (f32[512,256]{1,0:T(8,128)S(1)}, f32[512,256]{1,0:T(8,128)}, u32[]{:S(2)}) copy-start(f32[512,256]{1,0:T(8,128)} %fusion.7) | copy-start | bytes 1572868
  156.1 3.5 %copy-start.8 = (f32[512,256]{1,0:T(8,128)S(1)}, f32[512,256]{1,0:T(8,128)}, u32[]{:S(2)}) copy-start(f32[512,256]{1,0:T(8,128)} %fusion.10) | copy-start | bytes 1572868
  161.4 9.6 %copy-start.10 = (bf16[512,256]{1,0:T(8,128)(2,1)S(1)}, bf16[512,256]{1,0:T(8,128)(2,1)}, u32[]{:S(2)}) copy-start(bf16[512,256]{1,0:T(8,128)(2,1)} %copy-done.9) | copy-start | bytes 786436
  169.7 5.8 %collective-permute-start = (bf16[30,512]{1,0:T(8,128)(2,1)S(1)}, bf16[30,512]{1,0:T(8,128)(2,1)S(1)}, u32[]{:S(2)}, u32[]{:S(2)}) collective-permute-start(bf16[30,512]{1,0:T(8,128)(2,1)S(1)} %slice.713), channel_id=1, source_target_pairs={{4,0},{8,4},{12,8},{16,12},{20,16},{24,20},{28,24},{5,1},{9,5},{13... | collective-permute-start | bytes 92168 | tf_op jit(solution)/shard_map/ppermute | solution.py:12
Sparse Core Ops, SparseCore 0:
  37.2 21.5 all-gather.2
  63.5 21.6 all-gather.4
  91.6 31.1 reduce-scatter.2
  155.4 87.0 reduce-scatter.4
where the time goes:
time: 250 us; the launch traced here: 249 us
  waiting for transfers between devices  123 us (49%)
  blocking collectives  59.1 us (24%)
  matrix products  23.1 us (9%)
  local copies, waits for them, and re-layouts  15.8 us (6%)
  between operations  14 us (6%)
  other arithmetic  7.12 us (3%)
  starting transfers between devices  6.97 us (3%)
    reduce_scatter x1, waiting for transfers between devices, on_device(): lax.psum_scatter(lax.dot_general(mix_grad, activated, (((0,), (0,)), ((),...  65.6 us
    reduce_scatter x1, waiting for transfers between devices, on_device(): lax.psum_scatter(partial_value.astype(jnp.bfloat16), 'tp', scatter_dimens...  31.3 us
    all_to_all x1, blocking collectives, on_device(): lax.all_to_all(send_rows, 'sp', split_axis=0, concat_axis=0, tiled=True)  21.7 us
    all_to_all x1, blocking collectives, on_device(): lax.all_to_all(send_cot, 'sp', split_axis=0, concat_axis=0, tiled=True)  17.5 us
    all_gather x1, waiting for transfers between devices, on_device(): lax.all_gather(cot_slice, 'tp', axis=1, tiled=True)  16.7 us
    all_to_all x1, waiting for transfers between devices, on_device(): lax.all_to_all(back_slice, 'sp', split_axis=0, concat_axis=0, tiled=True)  8.16 us
    psum x1, blocking collectives, on_device(): dot_sum = lax.psum(jnp.sum(conv_vals * scaled, axis=1), 'tp')  7.21 us
    all_gather x1, blocking collectives, on_device(): mix_grad = lax.all_gather(mix_part, 'tp', axis=1, tiled=True)  6.68 us
  transfers between devices with their start and end apart: 6, of which 5 were waited for; matrix products, arithmetic and copies ran while one was open for 10% of the time, Pallas kernels for 0%

commit v1 on v0

--- a/solution.py
+++ b/solution.py
@@ -1,6 +1,10 @@
+import functools
+
 import jax
 import jax.numpy as jnp
 from jax import lax
+from jax.experimental import pallas as pl
+from jax.experimental.pallas import tpu as pltpu
 from jax.sharding import PartitionSpec as P
 
 norm_epsilon = 1e-05
@@ -129,6 +133,398 @@
     return (gate_g[None], up_g[None], down_g[None], proj_grad, gated_grad)
 
 
+VMEM = pl.BlockSpec(memory_space=pltpu.VMEM)
+DMA = pltpu.SemaphoreType.DMA
+MESH = pl.DeviceIdType.MESH
+
+
+def greet(peers):
+    barrier = pltpu.get_barrier_semaphore()
+    for peer in peers:
+        pl.semaphore_signal(barrier, inc=1, device_id=peer, device_id_type=MESH)
+    pl.semaphore_wait(barrier, len(peers))
+
+
+def send(src, dst, send_sem, recv_sem, device):
+    return pltpu.make_async_remote_copy(
+        src_ref=src,
+        dst_ref=dst,
+        send_sem=send_sem,
+        recv_sem=recv_sem,
+        device_id=device,
+        device_id_type=MESH,
+    )
+
+
+def places():
+    me, q = lax.axis_index("sp"), lax.axis_index("tp")
+    twin = q + 1 - 2 * (q % 2)
+    across = (q + 2) % 4
+    return me, q, twin, across
+
+
+def params(number):
+    return pltpu.CompilerParams(collective_id=number, has_side_effects=True)
+
+
+def span(index, size):
+    return pl.ds(pl.multiple_of(index * size, size), size)
+
+
+def dispatch_kernel(n, s_ref, sq_ref, xc_ref, sqs_ref, own_sem, a_s, a_r, t_s, t_r, x_s, x_r, f_s, f_r, q_s, q_r):
+    me, q, twin, across = places()
+    rows, cols = s_ref.shape[2], s_ref.shape[3]
+    twin_across = (twin + 2) % 4
+    greet([((me + j) % n, q) for j in range(1, n)] + [(me, twin), (me, across), (me, twin_across)])
+    order = [n // 2] + [j for d in range(1, n // 2) for j in (n // 2 - d, n // 2 + d)]
+    pending = []
+    for j in order:
+        d = (me + j) % n
+        c = send(s_ref.at[d], xc_ref.at[:, span(me, rows), span(q, cols)], a_s.at[j], a_r.at[j], (d, q))
+        c.start()
+        pending.append(c)
+    own = pltpu.make_async_copy(s_ref.at[me], xc_ref.at[:, span(me, rows), span(q, cols)], own_sem)
+    own.start()
+    own_sq = pltpu.make_async_copy(sq_ref, sqs_ref.at[q], q_s.at[3])
+    own_sq.start()
+    small = []
+    for k, peer in enumerate((twin, across, twin_across)):
+        c = send(sq_ref, sqs_ref.at[q], q_s.at[k], q_r.at[k], (me, peer))
+        c.start()
+        small.append(c)
+
+    def block(j, quarter):
+        return xc_ref.at[:, span((me + n - j) % n, rows), span(quarter, cols)]
+
+    last = []
+
+    def relay(j):
+        arrived = send(block(j, across), block(j, across), x_s.at[j], x_r.at[j], (me, across))
+        arrived.wait_recv()
+        c = send(block(j, across), block(j, across), f_s.at[j], f_r.at[j], (me, twin))
+        c.start()
+        last.append(c)
+        pending.append(c)
+
+    queue = [0] + order
+    for at, j in enumerate(queue):
+        if j == 0:
+            own.wait()
+        else:
+            send(s_ref.at[me], block(j, q), a_s.at[j], a_r.at[j], (me, q)).wait_recv()
+        c = send(block(j, q), block(j, q), x_s.at[j], x_r.at[j], (me, across))
+        c.start()
+        pending.append(c)
+        c = send(block(j, q), block(j, q), t_s.at[j], t_r.at[j], (me, twin))
+        c.start()
+        pending.append(c)
+        last.append(c)
+        if at >= 1:
+            relay(queue[at - 1])
+    relay(queue[-1])
+    for c in last:
+        c.wait_recv()
+    for c in small:
+        c.wait()
+    own_sq.wait()
+    for c in pending:
+        c.wait_send()
+
+
+def return_kernel(n, p_ref, act_ref, ret_ref, all_ref, d_r, sx, rx, back, d1_s, d1_r, x_s, x_r, a_s, a_r, o_sem,
+                  up_s, up_r, dn_s, dn_r, y_s, y_r):
+    me, q, twin, across = places()
+    rows, cols = ret_ref.shape[0] // n, ret_ref.shape[1]
+    tokens = act_ref.shape[0]
+    level, side = me // 2, me % 2
+    mate = me + 1 - 2 * side
+    levels = n // 2
+    below, above = (me + n - 2) % n, (me + 2) % n
+    greet([((me + j) % n, q) for j in range(1, n)] + [(me, twin), (me, across)])
+    twin_across = (twin + 2) % 4
+    order = [n // 2] + [j for d in range(1, n // 2) for j in (n // 2 - d, n // 2 + d)] + [0]
+    waits = []
+    firsts = {}
+    for j in order:
+        for k, quarter in enumerate((twin, twin_across)):
+            part = span((me + j) % n, rows)
+            c = send(p_ref.at[part, span(quarter, cols)], d_r.at[k, part], d1_s.at[k, j], d1_r.at[k, j], (me, twin))
+            c.start()
+            firsts[k, j] = c
+            waits.append(c)
+    own = pltpu.make_async_copy(act_ref, all_ref.at[span(me, tokens)], o_sem)
+    own.start()
+
+    def piece(lvl):
+        return all_ref.at[span((lvl + levels) % levels * 2 + side, tokens)]
+
+    def ways(t):
+        up = send(act_ref if t == 0 else piece(level - t), piece(level - t), up_s.at[t], up_r.at[t], (above, q))
+        dn = send(act_ref if t == 0 else piece(level + t), piece(level + t), dn_s.at[t], dn_r.at[t], (below, q))
+        return up, dn
+
+    def over(k, lvl):
+        src = act_ref if k == 0 else piece(lvl)
+        return send(src, piece(lvl), y_s.at[k], y_r.at[k], (mate, q))
+
+    def start_ways(t):
+        up, dn = ways(t)
+        pl.when(jnp.logical_and(level - t >= 0, level + 1 < levels))(up.start)
+        pl.when(jnp.logical_and(level + t < levels, level >= 1))(dn.start)
+
+    def take(t):
+        got_up = send(act_ref, piece(level - 1 - t), up_s.at[t], up_r.at[t], (above, q))
+        got_dn = send(act_ref, piece(level + 1 + t), dn_s.at[t], dn_r.at[t], (below, q))
+
+        @pl.when(level - 1 - t >= 0)
+        def _():
+            got_up.wait_recv()
+            over(1 + t, level - 1 - t).start()
+
+        @pl.when(level + 1 + t < levels)
+        def _():
+            got_dn.wait_recv()
+            over(levels + t, level + 1 + t).start()
+
+    start_ways(0)
+    over(0, level).start()
+
+    def first(j):
+        part = span((me + j) % n, rows)
+        for k in range(2):
+            firsts[k, j].wait_recv()
+        near = p_ref[part, span(across, cols)].astype(jnp.float32) + d_r[1, part].astype(jnp.float32)
+        sx[part] = near.astype(jnp.bfloat16)
+        c = send(sx.at[part], rx.at[part], x_s.at[j], x_r.at[j], (me, across))
+        c.start()
+        waits.append(c)
+        return c
+
+    outgoing = {}
+
+    def second(j, c):
+        part = span((me + j) % n, rows)
+        c.wait_recv()
+        total = p_ref[part, span(q, cols)].astype(jnp.float32) + d_r[0, part].astype(jnp.float32)
+        total = (total + rx[part].astype(jnp.float32)).astype(jnp.bfloat16)
+        if j == 0:
+            ret_ref[part] = total
+        else:
+            back[part] = total
+            a = send(back.at[part], ret_ref.at[span(me, rows)], a_s.at[j], a_r.at[j], ((me + j) % n, q))
+            a.start()
+            outgoing[j] = a
+            waits.append(a)
+
+    crossing = [first(j) for j in order]
+    take(0)
+    start_ways(1)
+    for at, j in enumerate(order):
+        second(j, crossing[at])
+        if at == 2:
+            take(1)
+            start_ways(2)
+        if at == 5:
+            take(2)
+    for j in order[:-1]:
+        got = send(back.at[span(me, rows)], ret_ref.at[span((me + n - j) % n, rows)], a_s.at[j], a_r.at[j], (me, q))
+        got.wait_recv()
+    for c in waits:
+        c.wait_send()
+    own.wait()
+
+    def other(lvl):
+        return all_ref.at[span((lvl + levels) % levels * 2 + 1 - side, tokens)]
+
+    for t in range(levels - 1):
+        up, dn = ways(t)
+        pl.when(jnp.logical_and(level - t >= 0, level + 1 < levels))(up.wait_send)
+        pl.when(jnp.logical_and(level + t < levels, level >= 1))(dn.wait_send)
+    for k in range(2 * levels - 1):
+        lvl = level - k if k < levels else level + k - levels + 1
+        here = lvl >= 0 if k < levels else lvl < levels
+
+        @pl.when(here)
+        def _():
+            over(k, lvl).wait_send()
+            send(act_ref, other(lvl), y_s.at[k], y_r.at[k], (mate, q)).wait_recv()
+
+
+def tail_kernel(n, mix_ref, act_ref, w_ref, conv_ref, inv_ref, gain_ref, taps_ref, gated_ref, proj_ref,
+                mg, pr, ext, halo, dots, m_s, m_r, f_s, f_r, a_s, a_r, o_sem, d_s, d_r, h_s, h_r):
+    me, q, twin, across = places()
+    twin_across = (twin + 2) % 4
+    tokens, cols = mix_ref.shape
+    block = proj_ref.shape[0]
+    reach = taps_ref.shape[0] - 1
+    pad = halo.shape[1]
+    greet([((me + j) % n, q) for j in range(1, n)] + [(me, twin), (me, across), (me, twin_across)])
+    to_x = send(mix_ref, mg.at[:, span(q, cols)], m_s.at[0], m_r.at[0], (me, across))
+    to_x.start()
+    to_twin = send(mix_ref, mg.at[:, span(q, cols)], m_s.at[1], m_r.at[1], (me, twin))
+    to_twin.start()
+    own = pltpu.make_async_copy(mix_ref, mg.at[:, span(q, cols)], o_sem.at[0])
+    own.start()
+    conv = conv_ref[...].astype(jnp.float32)
+    inv = inv_ref[...]
+    gain = gain_ref[...]
+    normed = conv * inv * gain
+    sig = jax.nn.sigmoid(normed)
+    slope = sig * (1.0 + normed * (1.0 - sig)) * gain
+    to_x.wait_recv()
+    relay = send(mg.at[:, span(across, cols)], mg.at[:, span(across, cols)], f_s, f_r, (me, twin))
+    relay.start()
+    to_twin.wait_recv()
+    relay.wait_recv()
+    own.wait()
+    pending = [to_x, to_twin, relay]
+    incoming = []
+    order = [n // 2] + [j for d in range(1, n // 2) for j in (n // 2 - d, n // 2 + d)]
+    for j in order:
+        d = (me + j) % n
+        c = send(mg.at[:, span(d, block)], pr.at[span(me, tokens)], a_s.at[j], a_r.at[j], (d, q))
+        c.start()
+        pending.append(c)
+        incoming.append(
+            send(mg.at[:, span(d, block)], pr.at[span((me + n - j) % n, tokens)], a_s.at[j], a_r.at[j], (d, q))
+        )
+    mine = pltpu.make_async_copy(mg.at[:, span(me, block)], pr.at[span(me, tokens)], o_sem.at[1])
+    mine.start()
+    into = lax.dot_general(mg[...], w_ref[...], (((1,), (1,)), ((), ())), preferred_element_type=jnp.float32)
+    scaled = into * slope
+    dot = jnp.sum(conv * scaled, axis=1, keepdims=True)
+    dots[0] = jnp.broadcast_to(dot, dots.shape[1:])
+    small = []
+    for k, peer in enumerate((twin, across, twin_across)):
+        c = send(dots.at[0], dots.at[k + 1], d_s.at[k], d_r.at[k], (me, peer))
+        c.start()
+        small.append(c)
+    ext[pl.ds(0, tokens)] = inv * scaled
+    for c in small:
+        c.wait()
+    total = dots[0] + dots[1] + dots[2] + dots[3]
+    total = total[:, :1]
+    grad = ext[pl.ds(0, tokens)] - conv * (inv * inv * inv * (total / (cols * 4)))
+    ext[pl.ds(0, tokens)] = grad
+    halo[0] = grad[:pad].astype(jnp.bfloat16)
+    shift = send(halo.at[0], halo.at[1], h_s, h_r, ((me + n - 1) % n, q))
+    pl.when(me > 0)(shift.start)
+
+    mine.wait()
+    for c in incoming:
+        c.wait_recv()
+    proj_ref[...] = lax.dot_general(
+        pr[...], act_ref[...], (((0,), (0,)), ((), ())), preferred_element_type=jnp.float32
+    )
+
+    @pl.when(me < n - 1)
+    def _():
+        shift.wait_recv()
+        ext[pl.ds(tokens, pad)] = halo[1].astype(jnp.float32)
+
+    @pl.when(me == n - 1)
+    def _():
+        ext[pl.ds(tokens, pad)] = jnp.zeros((pad, cols), jnp.float32)
+
+    pl.when(me > 0)(shift.wait_send)
+    step = 128
+    for low in range(0, cols, step):
+        band = pl.ds(low, step)
+        acc = taps_ref[pl.ds(0, 1), band] * ext[pl.ds(0, tokens), band]
+        for tap in range(1, reach + 1):
+            acc = acc + taps_ref[pl.ds(tap, 1), band] * ext[pl.ds(tap, tokens), band]
+        gated_ref[:, band] = acc
+    for c in pending:
+        c.wait_send()
+
+
+def near_plan(mixer_out, conv_out, out_cot, routes, route_weight, gate_weight, up_weight, down_weight, out_weight,
+              norm_gain, conv_taps):
+    tokens_here, model_width = out_cot.shape
+    n = lax.axis_size("sp")
+    capacity = 2 * tokens_here * routes.shape[1] // n
+    quarter = conv_out.shape[1]
+    first_col = lax.axis_index("tp") * quarter
+    bf16, f32 = jnp.bfloat16, jnp.float32
+    experts = jnp.arange(n, dtype=jnp.int32)[:, None, None]
+    named = routes.T[None] == experts
+    member = jnp.any(named, axis=1)
+    weight_of = jnp.sum(jnp.where(named, route_weight.T[None], 0.0), axis=1)
+    earlier = jnp.arange(tokens_here)[:, None] < jnp.arange(tokens_here)[None, :]
+    rank = jnp.dot(member.astype(bf16), earlier.astype(bf16), preferred_element_type=f32).astype(jnp.int32)
+    chosen = (rank[:, None, :] == jnp.arange(capacity)[None, :, None]) & member[:, None, :]
+    select = chosen.astype(bf16).reshape(n * capacity, tokens_here)
+    slot_weight = jnp.sum(jnp.where(chosen, weight_of[:, None, :], 0.0), axis=2)
+    own_x = lax.dynamic_slice_in_dim(mixer_out, first_col, quarter, 1)
+    own_cot = lax.dynamic_slice_in_dim(out_cot, first_col, quarter, 1)
+    rows = jnp.dot(select, own_x, preferred_element_type=f32).astype(bf16)
+    cots = jnp.dot(select, own_cot, preferred_element_type=f32) * slot_weight.reshape(-1, 1)
+    packed = jnp.stack(
+        [rows.reshape(n, capacity, quarter), cots.astype(bf16).reshape(n, capacity, quarter)], axis=1
+    )
+    conv_vals = conv_out.astype(f32)
+    squares = jnp.sum(conv_vals * conv_vals, axis=1)
+    squares = jnp.broadcast_to(squares[None, :], (8, tokens_here))
+    total_rows = n * capacity
+    shape = jax.ShapeDtypeStruct
+    x_and_cot, all_squares = pl.pallas_call(
+        functools.partial(dispatch_kernel, n),
+        out_shape=(shape((2, total_rows, model_width), bf16), shape((4, 8, tokens_here), f32)),
+        in_specs=[VMEM] * 2,
+        out_specs=(VMEM, VMEM),
+        scratch_shapes=[DMA] + [DMA((n,))] * 8 + [DMA((4,))] * 2,
+        compiler_params=params(0),
+        name="dispatch",
+    )(packed, squares)
+    inv_rms = lax.rsqrt(jnp.sum(all_squares[:, 0], axis=0) / model_width + norm_epsilon)[:, None]
+    normed = conv_vals * inv_rms * norm_gain[None, :]
+    activated = (normed * jax.nn.sigmoid(normed)).astype(bf16)
+    gate_g, up_g, down_g, partial_value = expert_backward(
+        x_and_cot[0], x_and_cot[1], gate_weight[0], up_weight[0], down_weight[0]
+    )
+    levels = n // 2
+    returned, act_all = pl.pallas_call(
+        functools.partial(return_kernel, n),
+        out_shape=(shape((total_rows, quarter), bf16), shape((n * tokens_here, quarter), bf16)),
+        in_specs=[VMEM] * 2,
+        out_specs=(VMEM, VMEM),
+        scratch_shapes=[pltpu.VMEM((2, total_rows, quarter), bf16)]
+        + [pltpu.VMEM((total_rows, quarter), bf16)] * 3
+        + [DMA((2, n))] * 2
+        + [DMA((n,))] * 4
+        + [DMA]
+        + [DMA((levels,))] * 4
+        + [DMA((2 * levels,))] * 2,
+        compiler_params=params(1),
+        name="give_back",
+    )(partial_value.astype(bf16), activated)
+    summed = lax.dot_general(select, returned, (((0,), (0,)), ((), ())), preferred_element_type=f32)
+    mix_part = (own_cot.astype(f32) + summed).astype(bf16)
+    pad = -(-(conv_taps.shape[0] - 1) // 16) * 16
+    gated_grad, proj_grad = pl.pallas_call(
+        functools.partial(tail_kernel, n),
+        out_shape=(shape((tokens_here, quarter), f32), shape((model_width // n, quarter), f32)),
+        in_specs=[VMEM] * 7,
+        out_specs=(VMEM, VMEM),
+        scratch_shapes=[
+            pltpu.VMEM((tokens_here, model_width), bf16),
+            pltpu.VMEM((n * tokens_here, model_width // n), bf16),
+            pltpu.VMEM((tokens_here + pad, quarter), f32),
+            pltpu.VMEM((2, pad, quarter), bf16),
+            pltpu.VMEM((4, tokens_here, 128), f32),
+            DMA((2,)), DMA((2,)), DMA, DMA, DMA((n,)), DMA((n,)), DMA((2,)), DMA((3,)), DMA((3,)), DMA, DMA,
+        ],
+        compiler_params=params(2),
+        name="tail",
+    )(mix_part, act_all, out_weight, conv_out, inv_rms, norm_gain[None, :], conv_taps)
+    return (gate_g[None], up_g[None], down_g[None], proj_grad, gated_grad)
+
+
+def either_plan(*arrays):
+    near = lax.axis_size("tp") == 4 and lax.axis_size("sp") in (4, 8)
+    return near_plan(*arrays) if near else on_device(*arrays)
+
+
 def solution(mesh):
     placed = (
         P("sp", None),
@@ -144,7 +540,7 @@
         P(None, "tp"),
     )
     return jax.shard_map(
-        on_device,
+        either_plan,
         mesh=mesh,
         in_specs=placed,
         out_specs=(

time: 250 us -> 135 us (0.54)
  waiting for transfers between devices: 123 us -> 0 us
  Pallas kernels: 0 us -> 105 us
  blocking collectives: 59.1 us -> 0 us
  between operations: 14 us -> 0.78 us
  local copies, waits for them, and re-layouts: 15.8 us -> 5.89 us
  starting transfers between devices: 6.97 us -> 0 us
  matrix products: 23.1 us -> 16.6 us
    pallas_call x0 -> x3, Pallas kernels: none -> 105 us  [the longest x1 47.9 us: near_plan(): pl.pallas_call(functools.partial(dispatch_kernel, n), out_shape=(shape((2...]
    reduce_scatter x2 -> x0, waiting for transfers between devices: 96.9 us -> none  [the longest x1 65.6 us: on_device(): lax.psum_scatter(lax.dot_general(mix_grad, activated, (((0,), (0,)), ((),...]
    all_to_all x2 -> x0, blocking collectives: 39.2 us -> none  [the longest x1 21.7 us: on_device(): lax.all_to_all(send_rows, 'sp', split_axis=0, concat_axis=0, tiled=True)]
    all_gather x2 -> x0, waiting for transfers between devices: 16.7 us -> none  [the longest x1 16.7 us: on_device(): lax.all_gather(cot_slice, 'tp', axis=1, tiled=True)]
    psum x2 -> x0, blocking collectives: 13.2 us -> none  [the longest x1 7.21 us: on_device(): dot_sum = lax.psum(jnp.sum(conv_vals * scaled, axis=1), 'tp')]
    all_to_all x1 -> x0, waiting for transfers between devices: 8.16 us -> none  [on_device(): lax.all_to_all(back_slice, 'sp', split_axis=0, concat_axis=0, tiled=True)]
    all_gather x1 -> x0, blocking collectives: 6.68 us -> none  [on_device(): mix_grad = lax.all_gather(mix_part, 'tp', axis=1, tiled=True)]
    mul x5 -> x1, local copies, waits for them, and re-layouts: 6.42 us -> 0.08 us  [near_plan(): jnp.dot(select, own_cot, preferred_element_type=f32)]
  transfers between devices with their start and end apart: 6 -> 0, of which waited for: 5 -> 0; matrix products, arithmetic and copies ran while one was open for 10% -> 0% of each run, Pallas kernels for 0% -> 0%
where the time goes in v1:
time: 135 us; the launch traced here: 134 us
  Pallas kernels  105 us (78%)
  matrix products  16.6 us (12%)
  local copies, waits for them, and re-layouts  5.89 us (4%)
  other arithmetic  5.46 us (4%)
    pallas_call x1, Pallas kernels, near_plan(): pl.pallas_call(functools.partial(dispatch_kernel, n), out_shape=(shape((2...  47.9 us
    pallas_call x1, Pallas kernels, near_plan(): pl.pallas_call(functools.partial(return_kernel, n), out_shape=(shape((tot...  32.9 us
    pallas_call x1, Pallas kernels, near_plan(): pl.pallas_call(functools.partial(tail_kernel, n), out_shape=(shape((token...  24 us
    unnamed x14, local copies, waits for them, and re-layouts  4.39 us

profile of v1, /device:TPU:0, one launch (start us, length us, event | category | flops | bytes accessed | tf_op | source)
XLA Modules:
  0.0 133.6 jit_solution(3704133177083674078)
XLA Ops:
  0.6 0.0 copy-start
  0.7 0.1 eq.43
  0.7 0.8 fusion.39
  1.5 0.1 convolution_convert_fusion.4
  1.6 0.1 fusion.36
  1.8 0.7 select_reduce_fusion.1
  2.5 0.1 select_reduce_fusion
  2.6 0.1 mul.60
  2.7 1.2 fusion.18
  3.9 1.2 convolution_convert_fusion.3
  5.1 1.1 pad_maximum_fusion.s_ref
  6.2 1.1 fusion.26
  7.3 0.6 broadcast_in_dim.57.sq_ref
  7.9 47.9 %dispatch.1 = (bf16[2,512,2048]{2,1,0:T(8,128)(2,1)}, f32[4,8,128]{2,1,0:T(8,128)}) custom-call(bf16[8,2,64,512]{3,2,1,0:T(8,128)(2,1)} %pad_maximum_fusion.s_ref, f32[8,128]{1,0:T(8,128)} %broadcast_in_dim.57.sq_ref), custom_call_target="tpu_custom_call" | custom-call | tf_op jit(solution)/shard_map/dispatch/pallas_call | solution.py:470
  55.8 2.5 %fusion.8 = f32[512,256]{1,0:T(8,128)S(1)} fusion(bf16[2,512,2048]{2,1,0:T(8,128)(2,1)} %get-tuple-element.11, bf16[1,2048,256]{2,1,0:T(8,128)(2,1)S(1)} %copy-done), kind=kOutput, calls=%fused_computation.12 | convolution fusion | flops 536870912 | bytes 3670016 | tf_op jit(solution)/shard_map/dot_general | solution.py:20
  58.2 0.3 copy-done.4
  58.6 0.7 fusion.10
  59.3 0.5 copy-done.5
  59.8 0.8 multiply_convert_fusion.1
  60.6 1.7 %fusion = bf16[1,2048,256]{2,1,0:T(8,128)(2,1)} fusion(bf16[512,256]{1,0:T(8,128)(2,1)S(1)} %get-tuple-element.18, bf16[2,512,2048]{2,1,0:T(8,128)(2,1)S(1)} %copy-done.4), kind=kOutput, calls=%fused_computation.4 | convolution fusion | flops 537395200 | bytes 3407872 | tf_op jit(solution)/shard_map/dot_general | solution.py:34
  62.4 1.8 %fusion.1 = bf16[1,2048,256]{2,1,0:T(8,128)(2,1)} fusion(bf16[512,256]{1,0:T(8,128)(2,1)S(1)} %get-tuple-element.17, bf16[2,512,2048]{2,1,0:T(8,128)(2,1)S(1)} %copy-done.4), kind=kOutput, calls=%fused_computation.5 | convolution fusion | flops 537395200 | bytes 3407872 | tf_op jit(solution)/shard_map/dot_general | solution.py:37
  64.1 1.8 %fusion.2 = bf16[1,256,2048]{2,1,0:T(8,128)(2,1)} fusion(bf16[2,512,2048]{2,1,0:T(8,128)(2,1)S(1)} %copy-done.4, f32[512,256]{1,0:T(8,128)S(1)} %fusion.10, f32[512,256]{1,0:T(8,128)S(1)} %fusion.8), kind=kOutput, calls=%fused_computation.6 | convolution fusion | flops 538181632 | bytes 4194304 | tf_op jit(solution)/shard_map/dot_general | solution.py:24
  65.9 0.7 fusion.20
  66.7 2.1 %add_convert_fusion.p_ref = bf16[512,2048]{1,0:T(8,128)(2,1)} fusion(f32[512,2048]{1,0:T(8,128)S(1)} %fusion.20, bf16[512,256]{1,0:T(8,128)(2,1)S(1)} %get-tuple-element.17, bf16[1,2048,256]{2,1,0:T(8,128)(2,1)S(1)} %copy-done.2), kind=kOutput, calls=%fused_computation | convolution fusion | flops 538968064 | bytes 7602176 | tf_op jit(solution)/shard_map/dot_general | solution.py:43
  68.8 0.7 slice_reduce_fusion
  69.5 0.8 fusion.33.act_ref
  70.3 32.9 %give_back.1 = (bf16[512,512]{1,0:T(8,128)(2,1)}, bf16[1024,512]{1,0:T(8,128)(2,1)}) custom-call(bf16[512,2048]{1,0:T(8,128)(2,1)} %add_convert_fusion.p_ref, bf16[128,512]{1,0:T(8,128)(2,1)} %fusion.33.act_ref), custom_call_target="tpu_custom_call" | custom-call | tf_op jit(solution)/shard_map/give_back/pallas_call | solution.py:486
  103.3 2.0 %fusion.19.mix_ref = bf16[128,512]{1,0:T(8,128)(2,1)} fusion(pred[512,128]{1,0:T(32,128)(4,1)S(1)} %fusion.36, bf16[512,512]{1,0:T(8,128)(2,1)} %get-tuple-element.13, bf16[128,2048]{1,0:T(8,128)(2,1)} %param.13, s32[]{:T(128)S(6)} %select_n.12), kind=kOutput, calls=%fused_computation.26 | convolution fusion | flops 67305472 | bytes 851972 | tf_op jit(solution)/shard_map/dot_general | solution.py:501
  105.3 0.7 copy.17.inv_ref
  106.0 24.0 %tail.1 = (f32[128,512]{1,0:T(8,128)}, f32[256,512]{1,0:T(8,128)}) custom-call(bf16[128,512]{1,0:T(8,128)(2,1)} %fusion.19.mix_ref, bf16[1024,512]{1,0:T(8,128)(2,1)} %get-tuple-element.14.act_ref, bf16[512,2048]{1,0:T(8,128)(2,1)} %w_ref.1, bf16[128,512]{1,0:T(8,128)(2,1)} %conv_ref.1, f32[128,1]{1,0:T(8,128)} %copy.17.inv_ref, f32[1,512]{1,0:T(1,128)} %bitcast.61, ...), custom_call_target="tpu_custom_call" | custom-call | tf_op jit(solution)/shard_map/tail/pallas_call | solution.py:504
  130.0 1.9 %copy.24 = f32[256,512]{1,0:T(8,128)} copy(f32[256,512]{1,0:T(8,128)} %get-tuple-element.29) | data formatting | bytes 1048576
  131.9 1.7 %copy.25 = f32[128,512]{1,0:T(8,128)} copy(f32[128,512]{1,0:T(8,128)} %get-tuple-element.30) | data formatting | bytes 524288
  (11 shorter events, 0.0 us)
Async XLA Ops:
  0.6 55.1 %copy-start = (bf16[1,2048,256]{2,1,0:T(8,128)(2,1)S(1)}, bf16[1,2048,256]{2,1,0:T(8,128)(2,1)}, u32[]{:S(2)}) copy-start(bf16[1,2048,256]{2,1,0:T(8,128)(2,1)} %param.16) | copy-start | bytes 3145732
  6.2 52.1 %copy-start.2 = (bf16[1,2048,256]{2,1,0:T(8,128)(2,1)S(1)}, bf16[1,2048,256]{2,1,0:T(8,128)(2,1)}, u32[]{:S(2)}) copy-start(bf16[1,2048,256]{2,1,0:T(8,128)(2,1)} %param.17) | copy-start | bytes 3145732
  55.8 2.8 %copy-start.4 = (bf16[2,512,2048]{2,1,0:T(8,128)(2,1)S(1)}, bf16[2,512,2048]{2,1,0:T(8,128)(2,1)}, u32[]{:S(2)}) copy-start(bf16[2,512,2048]{2,1,0:T(8,128)(2,1)} %get-tuple-element.11) | copy-start | bytes 12582916
  58.6 1.2 copy-start.5
  66.6 2.9 %copy-start.1 = (bf16[128,512]{1,0:T(8,128)(2,1)S(1)}, bf16[128,512]{1,0:T(8,128)(2,1)}, u32[]{:S(2)}) copy-start(bf16[128,512]{1,0:T(8,128)(2,1)} %conv_ref.1) | copy-start | bytes 393220
  66.7 2.9 %copy-start.3 = (f32[512]{0:T(512)S(1)}, f32[512]{0:T(512)}, u32[]{:S(2)}) copy-start(f32[512]{0:T(512)} %param.20) | copy-start | bytes 6148

commit v2 on v0

--- a/solution.py
+++ b/solution.py
@@ -1,6 +1,10 @@
+import functools
+
 import jax
 import jax.numpy as jnp
 from jax import lax
+from jax.experimental import pallas as pl
+from jax.experimental.pallas import tpu as pltpu
 from jax.sharding import PartitionSpec as P
 
 norm_epsilon = 1e-05
@@ -129,6 +133,446 @@
     return (gate_g[None], up_g[None], down_g[None], proj_grad, gated_grad)
 
 
+VMEM = pl.BlockSpec(memory_space=pltpu.VMEM)
+DMA = pltpu.SemaphoreType.DMA
+MESH = pl.DeviceIdType.MESH
+
+
+def greet(peers):
+    barrier = pltpu.get_barrier_semaphore()
+    for peer in peers:
+        pl.semaphore_signal(barrier, inc=1, device_id=peer, device_id_type=MESH)
+    pl.semaphore_wait(barrier, len(peers))
+
+
+def send(src, dst, send_sem, recv_sem, device):
+    return pltpu.make_async_remote_copy(
+        src_ref=src,
+        dst_ref=dst,
+        send_sem=send_sem,
+        recv_sem=recv_sem,
+        device_id=device,
+        device_id_type=MESH,
+    )
+
+
+def places():
+    me, q = lax.axis_index("sp"), lax.axis_index("tp")
+    twin = q + 1 - 2 * (q % 2)
+    across = (q + 2) % 4
+    return me, q, twin, across
+
+
+def params(number):
+    return pltpu.CompilerParams(collective_id=number, has_side_effects=True)
+
+
+def span(index, size):
+    return pl.ds(pl.multiple_of(index * size, size), size)
+
+
+def toggled(value, bits):
+    power = 1
+    while power <= bits:
+        if bits & power:
+            value = value + power - 2 * power * ((value // power) % 2)
+        power *= 2
+    return value
+
+
+def as_row(column):
+    size = column.shape[0]
+    same = lax.broadcasted_iota(jnp.int32, (size, size), 0) == lax.broadcasted_iota(jnp.int32, (size, size), 1)
+    return jnp.sum(jnp.where(same, column, 0.0), axis=0, keepdims=True)
+
+
+def as_column(row):
+    size = row.shape[1]
+    same = lax.broadcasted_iota(jnp.int32, (size, size), 0) == lax.broadcasted_iota(jnp.int32, (size, size), 1)
+    return jnp.sum(jnp.where(same, row, 0.0), axis=1, keepdims=True)
+
+
+def dispatch_kernel(n, x_hbm, cot_hbm, routes_ref, weight_ref, conv_ref, xc_ref, sel_ref, sqs_ref,
+                    xq, cq, s_buf, codes, wts, in_sem, own_sem, a_s, a_r, t_s, t_r, x_s, x_r, f_s, f_r, q_s, q_r):
+    me, q, twin, across = places()
+    twin_across = (twin + 2) % 4
+    bf16, f32 = jnp.bfloat16, jnp.float32
+    tokens, cols = xq.shape
+    rows = s_buf.shape[2]
+    loads = [
+        pltpu.make_async_copy(x_hbm.at[:, span(q, cols)], xq, in_sem.at[0]),
+        pltpu.make_async_copy(cot_hbm.at[:, span(q, cols)], cq, in_sem.at[1]),
+    ]
+    for c in loads:
+        c.start()
+    barrier = pltpu.get_barrier_semaphore()
+    peers = [(toggled(me, j), q) for j in range(1, n)] + [(me, twin), (me, across), (me, twin_across)]
+    for peer in peers:
+        pl.semaphore_signal(barrier, inc=1, device_id=peer, device_id_type=MESH)
+    height = codes.shape[0]
+    which = lax.broadcasted_iota(jnp.int32, (height, tokens), 0)
+    member = jnp.zeros((height, tokens), f32)
+    weight_of = jnp.zeros((height, tokens), f32)
+    for k in range(routes_ref.shape[0]):
+        named = routes_ref[pl.ds(k, 1), :] == which
+        member = jnp.where(named, 1.0, member)
+        weight_of = jnp.where(named, weight_ref[pl.ds(k, 1), :], weight_of)
+    earlier = lax.broadcasted_iota(jnp.int32, (tokens, tokens), 0) < lax.broadcasted_iota(
+        jnp.int32, (tokens, tokens), 1
+    )
+    rank = jnp.dot(member.astype(bf16), jnp.where(earlier, 1.0, 0.0).astype(bf16), preferred_element_type=f32)
+    codes[...] = jnp.where(member > 0.5, rank, -1.0)
+    wts[...] = weight_of
+    conv = conv_ref[...].astype(f32)
+    squares = as_row(jnp.sum(conv * conv, axis=1, keepdims=True))
+    sqs_ref[q] = jnp.broadcast_to(squares, sqs_ref.shape[1:])
+    place = lax.broadcasted_iota(jnp.int32, (rows, tokens), 0).astype(f32)
+    for c in loads:
+        c.wait()
+    pending = []
+    for j in range(n):
+        d = toggled(me, j)
+        chosen = codes[pl.ds(d, 1), :] == place
+        select = jnp.where(chosen, 1.0, 0.0).astype(bf16)
+        scale = jnp.sum(jnp.where(chosen, wts[pl.ds(d, 1), :], 0.0), axis=1, keepdims=True)
+        sel_ref[span(d, rows), :] = select
+        s_buf[j, 0] = jnp.dot(select, xq[...], preferred_element_type=f32).astype(bf16)
+        s_buf[j, 1] = (jnp.dot(select, cq[...], preferred_element_type=f32) * scale).astype(bf16)
+        if j == 0:
+            pl.semaphore_wait(barrier, len(peers))
+            target = xc_ref.at[:, span(me, rows), span(q, cols)]
+            own = pltpu.make_async_copy(s_buf.at[0], target, own_sem)
+            own.start()
+            for part, (sem_s, sem_r, peer) in enumerate(((x_s, x_r, across), (t_s, t_r, twin))):
+                c = send(s_buf.at[0], target, sem_s.at[0], sem_r.at[0], (me, peer))
+                c.start()
+                pending.append(c)
+        else:
+            c = send(s_buf.at[j], xc_ref.at[:, span(me, rows), span(q, cols)], a_s.at[j], a_r.at[j], (d, q))
+            c.start()
+            pending.append(c)
+    last = [pending[1]]
+    small = []
+    for k, peer in enumerate((twin, across, twin_across)):
+        c = send(sqs_ref.at[q], sqs_ref.at[q], q_s.at[k], q_r.at[k], (me, peer))
+        c.start()
+        small.append(c)
+
+    def block(j, quarter):
+        return xc_ref.at[:, span(toggled(me, j), rows), span(quarter, cols)]
+
+    def relay(j):
+        c = send(block(j, across), block(j, across), f_s.at[j], f_r.at[j], (me, twin))
+        send(block(j, across), block(j, across), x_s.at[j], x_r.at[j], (me, across)).wait_recv()
+        c.start()
+        last.append(c)
+        pending.append(c)
+
+    for j in range(1, n):
+        send(s_buf.at[j], block(j, q), a_s.at[j], a_r.at[j], (me, q)).wait_recv()
+        c = send(block(j, q), block(j, q), x_s.at[j], x_r.at[j], (me, across))
+        c.start()
+        pending.append(c)
+        c = send(block(j, q), block(j, q), t_s.at[j], t_r.at[j], (me, twin))
+        c.start()
+        pending.append(c)
+        last.append(c)
+        relay(j - 1)
+    relay(n - 1)
+    own.wait()
+    for c in last:
+        c.wait_recv()
+    for c in small:
+        c.wait()
+    for c in pending:
+        c.wait_send()
+
+
+def rest_kernel(n, p_ref, sqs_ref, conv_ref, gain_ref, sel_ref, cot_hbm, w_ref, taps_ref, gated_ref, proj_ref,
+                act, all_ref, cq, d_r, sx, rx, back, ret, mg, pr, ext, halo, dots, in_sem, d1_s, d1_r, x_s, x_r,
+                a_s, a_r, o_sem, up_s, up_r, dn_s, dn_r, y_s, y_r, m_s, m_r, b_s, b_r, e_s, e_r, t_s, t_r, h_s, h_r):
+    me, q, twin, across = places()
+    twin_across = (twin + 2) % 4
+    bf16, f32 = jnp.bfloat16, jnp.float32
+    tokens, cols = conv_ref.shape
+    rows = ret.shape[0] // n
+    level, side = me // 2, me % 2
+    mate = me + 1 - 2 * side
+    levels = n // 2
+    below, above = (me + n - 2) % n, (me + 2) % n
+    before = (me + n - 1) % n
+    load = pltpu.make_async_copy(cot_hbm.at[:, span(q, cols)], cq, in_sem)
+    load.start()
+    greet([((me + j) % n, q) for j in range(1, n)] + [(me, twin), (me, across), (me, twin_across)])
+    order = list(range(n - 1, -1, -1))
+    waits = []
+    firsts = {}
+    for j in order:
+        for k, quarter in enumerate((twin_across, twin)):
+            part = span(toggled(me, j), rows)
+            c = send(p_ref.at[part, span(quarter, cols)], d_r.at[k, part], d1_s.at[k, j], d1_r.at[k, j], (me, twin))
+            c.start()
+            firsts[k, j] = c
+            waits.append(c)
+    conv = conv_ref[...].astype(f32)
+    gain = gain_ref[...]
+    power = as_column((sqs_ref[0] + sqs_ref[1] + sqs_ref[2] + sqs_ref[3])[:1])
+    inv = lax.rsqrt(power / (cols * 4) + norm_epsilon)
+    normed = conv * inv * gain
+    act[...] = (normed * jax.nn.sigmoid(normed)).astype(bf16)
+
+    def piece(lvl):
+        return all_ref.at[span((lvl + levels) % levels * 2 + side, tokens)]
+
+    def ways(t):
+        up = send(act if t == 0 else piece(level - t), piece(level - t), up_s.at[t], up_r.at[t], (above, q))
+        dn = send(act if t == 0 else piece(level + t), piece(level + t), dn_s.at[t], dn_r.at[t], (below, q))
+        return up, dn
+
+    def over(k, lvl):
+        src = act if k == 0 else piece(lvl)
+        return send(src, piece(lvl), y_s.at[k], y_r.at[k], (mate, q))
+
+    def start_ways(t):
+        up, dn = ways(t)
+        pl.when(jnp.logical_and(level - t >= 0, level + 1 < levels))(up.start)
+        pl.when(jnp.logical_and(level + t < levels, level >= 1))(dn.start)
+
+    def take(t):
+        got_up = send(act, piece(level - 1 - t), up_s.at[t], up_r.at[t], (above, q))
+        got_dn = send(act, piece(level + 1 + t), dn_s.at[t], dn_r.at[t], (below, q))
+
+        @pl.when(level - 1 - t >= 0)
+        def _():
+            got_up.wait_recv()
+            over(1 + t, level - 1 - t).start()
+
+        @pl.when(level + 1 + t < levels)
+        def _():
+            got_dn.wait_recv()
+            over(levels + t, level + 1 + t).start()
+
+    def first(j):
+        part = span(toggled(me, j), rows)
+        firsts[0, j].wait_recv()
+        near = p_ref[part, span(across, cols)].astype(f32) + d_r[0, part].astype(f32)
+        sx[part] = near.astype(bf16)
+        c = send(sx.at[part], rx.at[part], x_s.at[j], x_r.at[j], (me, across))
+        c.start()
+        waits.append(c)
+        return c
+
+    def second(j, c):
+        part = span(toggled(me, j), rows)
+        firsts[1, j].wait_recv()
+        total = p_ref[part, span(q, cols)].astype(f32) + d_r[1, part].astype(f32)
+        c.wait_recv()
+        total = (total + rx[part].astype(f32)).astype(bf16)
+        if j == 0:
+            ret[part] = total
+        else:
+            back[part] = total
+            out = send(back.at[part], ret.at[span(me, rows)], a_s.at[j], a_r.at[j], (toggled(me, j), q))
+            out.start()
+            waits.append(out)
+
+    crossing = [first(j) for j in order[:2]]
+    start_ways(0)
+    over(0, level).start()
+    own = pltpu.make_async_copy(act, all_ref.at[span(me, tokens)], o_sem.at[0])
+    own.start()
+    crossing += [first(j) for j in order[2:]]
+    for at, j in enumerate(order):
+        second(j, crossing[at])
+        if at == 1:
+            take(0)
+            start_ways(1)
+        if at == 4:
+            take(1)
+            start_ways(2)
+    load.wait()
+    for j in order[:-1]:
+        got = send(back.at[span(me, rows)], ret.at[span(toggled(me, j), rows)], a_s.at[j], a_r.at[j], (me, q))
+        got.wait_recv()
+
+    summed = lax.dot_general(sel_ref[...], ret[...], (((0,), (0,)), ((), ())), preferred_element_type=f32)
+    mg[:, span(q, cols)] = (cq[...].astype(f32) + summed).astype(bf16)
+    mine = mg.at[:, span(q, cols)]
+    to_x = send(mine, mine, m_s.at[0], m_r.at[0], (me, across))
+    to_x.start()
+    to_twin = send(mine, mine, m_s.at[1], m_r.at[1], (me, twin))
+    to_twin.start()
+    take(2)
+    sig = jax.nn.sigmoid(normed)
+    slope = sig * (1.0 + normed * (1.0 - sig)) * gain
+    theirs = mg.at[:, span(across, cols)]
+    to_x.wait_recv()
+    relay = send(theirs, theirs, m_s.at[2], m_r.at[2], (me, twin))
+    relay.start()
+    to_twin.wait_recv()
+    relay.wait_recv()
+    waits += [to_x, to_twin, relay]
+    share, block = pr.shape[2], pr.shape[3]
+    incoming = []
+    for j in order[:-1]:
+        d = toggled(me, j)
+        c = send(mg.at[span(q, share), span(d, block)], pr.at[me, q], b_s.at[j], b_r.at[j], (d, q))
+        c.start()
+        waits.append(c)
+        incoming.append(send(mg.at[span(q, share), span(d, block)], pr.at[d, q], b_s.at[j], b_r.at[j], (d, q)))
+    kept = pltpu.make_async_copy(mg.at[span(q, share), span(me, block)], pr.at[me, q], o_sem.at[1])
+    kept.start()
+    into = lax.dot_general(mg[...], w_ref[...], (((1,), (1,)), ((), ())), preferred_element_type=f32)
+    scaled = into * slope
+    dots[0] = jnp.broadcast_to(as_row(jnp.sum(conv * scaled, axis=1, keepdims=True)), dots.shape[1:])
+    small = []
+    for k, peer in enumerate((twin, across, twin_across)):
+        c = send(dots.at[0], dots.at[k + 1], t_s.at[k], t_r.at[k], (me, peer))
+        c.start()
+        small.append(c)
+    ext[pl.ds(0, tokens)] = inv * scaled
+    kept.wait()
+    for c in incoming:
+        c.wait_recv()
+    spread = [
+        send(pr.at[:, q], pr.at[:, q], e_s.at[0], e_r.at[0], (me, across)),
+        send(pr.at[:, q], pr.at[:, q], e_s.at[1], e_r.at[1], (me, twin)),
+        send(pr.at[:, across], pr.at[:, across], e_s.at[2], e_r.at[2], (me, twin)),
+    ]
+    spread[0].start()
+    spread[1].start()
+    for c in small:
+        c.wait()
+    total = as_column((dots[0] + dots[1] + dots[2] + dots[3])[:1])
+    grad = ext[pl.ds(0, tokens)] - conv * (inv * inv * inv * (total / (cols * 4)))
+    ext[pl.ds(0, tokens)] = grad
+    pad = halo.shape[1]
+    halo[0] = grad[:pad].astype(bf16)
+    shift = send(halo.at[0], halo.at[1], h_s, h_r, (before, q))
+    pl.when(me > 0)(shift.start)
+    spread[0].wait_recv()
+    spread[2].start()
+
+    @pl.when(me < n - 1)
+    def _():
+        shift.wait_recv()
+        ext[pl.ds(tokens, pad)] = halo[1].astype(f32)
+
+    @pl.when(me == n - 1)
+    def _():
+        ext[pl.ds(tokens, pad)] = jnp.zeros((pad, cols), f32)
+
+    step = 128
+    for low in range(0, cols, step):
+        band = pl.ds(low, step)
+        acc = taps_ref[pl.ds(0, 1), band] * ext[pl.ds(0, tokens), band]
+        for tap in range(1, taps_ref.shape[0]):
+            acc = acc + taps_ref[pl.ds(tap, 1), band] * ext[pl.ds(tap, tokens), band]
+        gated_ref[:, band] = acc
+
+    def other(lvl):
+        return all_ref.at[span((lvl + levels) % levels * 2 + 1 - side, tokens)]
+
+    for t in range(levels - 1):
+        up, dn = ways(t)
+        pl.when(jnp.logical_and(level - t >= 0, level + 1 < levels))(up.wait_send)
+        pl.when(jnp.logical_and(level + t < levels, level >= 1))(dn.wait_send)
+    for k in range(2 * levels - 1):
+        lvl = level - k if k < levels else level + k - levels + 1
+        here = lvl >= 0 if k < levels else lvl < levels
+
+        @pl.when(here)
+        def _():
+            over(k, lvl).wait_send()
+            send(act, other(lvl), y_s.at[k], y_r.at[k], (mate, q)).wait_recv()
+
+    own.wait()
+    spread[1].wait_recv()
+    spread[2].wait_recv()
+    proj_ref[...] = lax.dot_general(
+        pr[...].reshape(n * tokens, block), all_ref[...], (((0,), (0,)), ((), ())), preferred_element_type=f32
+    )
+    pl.when(me > 0)(shift.wait_send)
+    for c in spread:
+        c.wait_send()
+    for c in waits:
+        c.wait_send()
+
+
+def near_plan(mixer_out, conv_out, out_cot, routes, route_weight, gate_weight, up_weight, down_weight, out_weight,
+              norm_gain, conv_taps):
+    tokens_here, model_width = out_cot.shape
+    n = lax.axis_size("sp")
+    capacity = 2 * tokens_here * routes.shape[1] // n
+    quarter = conv_out.shape[1]
+    bf16, f32 = jnp.bfloat16, jnp.float32
+    total_rows = n * capacity
+    shape = jax.ShapeDtypeStruct
+    anywhere = pl.BlockSpec(memory_space=pl.ANY)
+    height = -(-n // 16) * 16
+    x_and_cot, select, squares = pl.pallas_call(
+        functools.partial(dispatch_kernel, n),
+        out_shape=(
+            shape((2, total_rows, model_width), bf16),
+            shape((total_rows, tokens_here), bf16),
+            shape((4, 8, tokens_here), f32),
+        ),
+        in_specs=[anywhere] * 2 + [VMEM] * 3,
+        out_specs=(VMEM, VMEM, VMEM),
+        scratch_shapes=[pltpu.VMEM((tokens_here, quarter), bf16)] * 2
+        + [pltpu.VMEM((n, 2, capacity, quarter), bf16)]
+        + [pltpu.VMEM((height, tokens_here), f32)] * 2
+        + [DMA((2,)), DMA]
+        + [DMA((n,))] * 8
+        + [DMA((3,))] * 2,
+        compiler_params=params(0),
+        name="dispatch",
+    )(mixer_out, out_cot, routes.T, route_weight.T, conv_out)
+    gate_g, up_g, down_g, partial_value = expert_backward(
+        x_and_cot[0], x_and_cot[1], gate_weight[0], up_weight[0], down_weight[0]
+    )
+    levels = n // 2
+    pad = -(-(conv_taps.shape[0] - 1) // 16) * 16
+    gated_grad, proj_grad = pl.pallas_call(
+        functools.partial(rest_kernel, n),
+        out_shape=(shape((tokens_here, quarter), f32), shape((model_width // n, quarter), f32)),
+        in_specs=[VMEM] * 5 + [anywhere] + [VMEM] * 2,
+        out_specs=(VMEM, VMEM),
+        scratch_shapes=[
+            pltpu.VMEM((tokens_here, quarter), bf16),
+            pltpu.VMEM((n * tokens_here, quarter), bf16),
+            pltpu.VMEM((tokens_here, quarter), bf16),
+            pltpu.VMEM((2, total_rows, quarter), bf16),
+        ]
+        + [pltpu.VMEM((total_rows, quarter), bf16)] * 4
+        + [
+            pltpu.VMEM((tokens_here, model_width), bf16),
+            pltpu.VMEM((n, 4, tokens_here // 4, model_width // n), bf16),
+            pltpu.VMEM((tokens_here + pad, quarter), f32),
+            pltpu.VMEM((2, pad, quarter), bf16),
+            pltpu.VMEM((4, 8, tokens_here), f32),
+            DMA,
+        ]
+        + [DMA((2, n))] * 2
+        + [DMA((n,))] * 4
+        + [DMA((2,))]
+        + [DMA((levels,))] * 4
+        + [DMA((2 * levels,))] * 2
+        + [DMA((3,))] * 2
+        + [DMA((n,))] * 2
+        + [DMA((3,))] * 4
+        + [DMA] * 2,
+        compiler_params=params(1),
+        name="rest",
+    )(partial_value.astype(bf16), squares, conv_out, norm_gain[None, :], select, out_cot, out_weight, conv_taps)
+    return (gate_g[None], up_g[None], down_g[None], proj_grad, gated_grad)
+
+
+def either_plan(*arrays):
+    near = lax.axis_size("tp") == 4 and lax.axis_size("sp") == 8
+    return near_plan(*arrays) if near else on_device(*arrays)
+
+
 def solution(mesh):
     placed = (
         P("sp", None),
@@ -144,7 +588,7 @@
         P(None, "tp"),
     )
     return jax.shard_map(
-        on_device,
+        either_plan,
         mesh=mesh,
         in_specs=placed,
         out_specs=(

time: 250 us -> 106 us (0.42)
  waiting for transfers between devices: 123 us -> 0 us
  Pallas kernels: 0 us -> 88.2 us
  blocking collectives: 59.1 us -> 0 us
  between operations: 14 us -> 0.72 us
  local copies, waits for them, and re-layouts: 15.8 us -> 4.38 us
  matrix products: 23.1 us -> 12.1 us
  other arithmetic: 7.12 us -> 0 us
  starting transfers between devices: 6.97 us -> 0 us
    reduce_scatter x2 -> x0, waiting for transfers between devices: 96.9 us -> none  [the longest x1 65.6 us: on_device(): lax.psum_scatter(lax.dot_general(mix_grad, activated, (((0,), (0,)), ((),...]
    pallas_call x0 -> x2, Pallas kernels: none -> 88.2 us  [the longest x1 49.1 us: near_plan(): pl.pallas_call(functools.partial(rest_kernel, n), out_shape=(shape((token...]
    all_to_all x2 -> x0, blocking collectives: 39.2 us -> none  [the longest x1 21.7 us: on_device(): lax.all_to_all(send_rows, 'sp', split_axis=0, concat_axis=0, tiled=True)]
    all_gather x2 -> x0, waiting for transfers between devices: 16.7 us -> none  [the longest x1 16.7 us: on_device(): lax.all_gather(cot_slice, 'tp', axis=1, tiled=True)]
    psum x2 -> x0, blocking collectives: 13.2 us -> none  [the longest x1 7.21 us: on_device(): dot_sum = lax.psum(jnp.sum(conv_vals * scaled, axis=1), 'tp')]
    all_to_all x1 -> x0, waiting for transfers between devices: 8.16 us -> none  [on_device(): lax.all_to_all(back_slice, 'sp', split_axis=0, concat_axis=0, tiled=True)]
    all_gather x1 -> x0, blocking collectives: 6.68 us -> none  [on_device(): mix_grad = lax.all_gather(mix_part, 'tp', axis=1, tiled=True)]
    mul x5 -> x0, local copies, waits for them, and re-layouts: 6.42 us -> none  [the longest x3 6.17 us: on_device(): route_weight[:, :, None] * out_cot[:, None, :].astype(jnp.float32)]
  transfers between devices with their start and end apart: 6 -> 0, of which waited for: 5 -> 0; matrix products, arithmetic and copies ran while one was open for 10% -> 0% of each run, Pallas kernels for 0% -> 0%
where the time goes in v2:
time: 106 us; the launch traced here: 105 us
  Pallas kernels  88.2 us (83%)
  matrix products  12.1 us (11%)
  local copies, waits for them, and re-layouts  4.38 us (4%)
    pallas_call x1, Pallas kernels, near_plan(): pl.pallas_call(functools.partial(rest_kernel, n), out_shape=(shape((token...  49.1 us
    pallas_call x1, Pallas kernels, near_plan(): pl.pallas_call(functools.partial(dispatch_kernel, n), out_shape=(shape((2...  39.1 us
    unnamed x10, local copies, waits for them, and re-layouts  4.38 us
    dot_general x1, matrix products, expert_backward(): pre_gate = jnp.dot(x_rows, w_gate, preferred_element_type=jnp.float32)  2.45 us

profile of v2, /device:TPU:0, one launch (start us, length us, event | category | flops | bytes accessed | tf_op | source)
XLA Modules:
  0.0 105.4 jit_solution(8208784588133135177)
XLA Ops:
  0.6 0.0 copy-start
  0.6 0.0 copy-start.1
  0.7 39.1 %dispatch.1 = (bf16[2,512,2048]{2,1,0:T(8,128)(2,1)}, bf16[512,128]{1,0:T(8,128)(2,1)}, f32[4,8,128]{2,1,0:T(8,128)}) custom-call(bf16[128,2048]{1,0:T(8,128)(2,1)} %x_hbm.1, bf16[128,2048]{1,0:T(8,128)(2,1)} %cot_hbm.3, s32[2,128]{1,0:T(2,128)} %bitcast.45, f32[2,128]{1,0:T(2,128)} %bitcast.46, bf16[128,512]{1,0:T(8,128)(2,1)} %conv_ref.3), custom_call_target="tpu_custom_call" | custom-call | tf_op jit(solution)/shard_map/dispatch/pallas_call | solution.py:513
  39.8 0.0 copy-start.2
  39.8 0.0 copy-done
  39.8 2.5 %fusion.8 = f32[512,256]{1,0:T(8,128)S(1)} fusion(bf16[2,512,2048]{2,1,0:T(8,128)(2,1)} %get-tuple-element.10, bf16[1,2048,256]{2,1,0:T(8,128)(2,1)S(1)} %copy-done), kind=kOutput, calls=%fused_computation.12 | convolution fusion | flops 536870912 | bytes 3670016 | tf_op jit(solution)/shard_map/dot_general | solution.py:20
  42.3 0.0 copy-done.1
  42.3 0.3 copy-done.2
  42.6 0.0 copy-start.3
  42.6 0.7 fusion.10
  43.3 0.5 copy-done.3
  43.8 0.8 multiply_convert_fusion.1
  44.7 1.8 %fusion.2 = bf16[1,256,2048]{2,1,0:T(8,128)(2,1)} fusion(bf16[2,512,2048]{2,1,0:T(8,128)(2,1)S(1)} %copy-done.2, f32[512,256]{1,0:T(8,128)S(1)} %fusion.10, f32[512,256]{1,0:T(8,128)S(1)} %fusion.8), kind=kOutput, calls=%fused_computation.6 | convolution fusion | flops 538181632 | bytes 4194304 | tf_op jit(solution)/shard_map/dot_general | solution.py:24
  46.4 1.8 %fusion.1 = bf16[1,2048,256]{2,1,0:T(8,128)(2,1)} fusion(bf16[512,256]{1,0:T(8,128)(2,1)S(1)} %get-tuple-element.15, bf16[2,512,2048]{2,1,0:T(8,128)(2,1)S(1)} %copy-done.2), kind=kOutput, calls=%fused_computation.5 | convolution fusion | flops 537395200 | bytes 3407872 | tf_op jit(solution)/shard_map/dot_general | solution.py:37
  48.2 1.7 %fusion = bf16[1,2048,256]{2,1,0:T(8,128)(2,1)} fusion(bf16[512,256]{1,0:T(8,128)(2,1)S(1)} %get-tuple-element.16, bf16[2,512,2048]{2,1,0:T(8,128)(2,1)S(1)} %copy-done.2), kind=kOutput, calls=%fused_computation.4 | convolution fusion | flops 537395200 | bytes 3407872 | tf_op jit(solution)/shard_map/dot_general | solution.py:34
  49.9 0.7 fusion.18
  50.7 2.1 %add_convert_fusion.p_ref = bf16[512,2048]{1,0:T(8,128)(2,1)} fusion(f32[512,2048]{1,0:T(8,128)S(1)} %fusion.18, bf16[512,256]{1,0:T(8,128)(2,1)S(1)} %get-tuple-element.15, bf16[1,2048,256]{2,1,0:T(8,128)(2,1)S(1)} %copy-done.1), kind=kOutput, calls=%fused_computation | convolution fusion | flops 538968064 | bytes 7602176 | tf_op jit(solution)/shard_map/dot_general | solution.py:43
  52.8 49.1 %rest.1 = (f32[128,512]{1,0:T(8,128)}, f32[256,512]{1,0:T(8,128)}) custom-call(bf16[512,2048]{1,0:T(8,128)(2,1)} %add_convert_fusion.p_ref, f32[4,8,128]{2,1,0:T(8,128)} %get-tuple-element.11.sqs_ref, bf16[128,512]{1,0:T(8,128)(2,1)} %conv_ref.3, f32[1,512]{1,0:T(1,128)} %bitcast.44, bf16[512,128]{1,0:T(8,128)(2,1)} %get-tuple-element.12.sel_ref, ...), custom_call_target="tpu_custom_call" | custom-call | tf_op jit(solution)/shard_map/rest/pallas_call | solution.py:536
  101.9 1.9 %copy.18 = f32[256,512]{1,0:T(8,128)} copy(f32[256,512]{1,0:T(8,128)} %get-tuple-element.25) | data formatting | bytes 1048576
  103.7 1.7 %copy.19 = f32[128,512]{1,0:T(8,128)} copy(f32[128,512]{1,0:T(8,128)} %get-tuple-element.26) | data formatting | bytes 524288
Async XLA Ops:
  0.6 39.2 %copy-start = (bf16[1,2048,256]{2,1,0:T(8,128)(2,1)S(1)}, bf16[1,2048,256]{2,1,0:T(8,128)(2,1)}, u32[]{:S(2)}) copy-start(bf16[1,2048,256]{2,1,0:T(8,128)(2,1)} %param.16) | copy-start | bytes 3145732
  0.6 41.6 %copy-start.1 = (bf16[1,2048,256]{2,1,0:T(8,128)(2,1)S(1)}, bf16[1,2048,256]{2,1,0:T(8,128)(2,1)}, u32[]{:S(2)}) copy-start(bf16[1,2048,256]{2,1,0:T(8,128)(2,1)} %param.17) | copy-start | bytes 3145732
  39.8 2.8 %copy-start.2 = (bf16[2,512,2048]{2,1,0:T(8,128)(2,1)S(1)}, bf16[2,512,2048]{2,1,0:T(8,128)(2,1)}, u32[]{:S(2)}) copy-start(bf16[2,512,2048]{2,1,0:T(8,128)(2,1)} %get-tuple-element.10) | copy-start | bytes 12582916
  42.6 1.2 %copy-start.3 = (bf16[1,256,2048]{2,1,0:T(8,128)(2,1)S(1)}, bf16[1,256,2048]{2,1,0:T(8,128)(2,1)}, u32[]{:S(2)}) copy-start(bf16[1,256,2048]{2,1,0:T(8,128)(2,1)} %param.18) | copy-start | bytes 3145732

commit v3 on v2

--- a/solution.py
+++ b/solution.py
@@ -288,8 +288,8 @@
         c.wait_send()
 
 
-def rest_kernel(n, p_ref, sqs_ref, conv_ref, gain_ref, sel_ref, cot_hbm, w_ref, taps_ref, gated_ref, proj_ref,
-                act, all_ref, cq, d_r, sx, rx, back, ret, mg, pr, ext, halo, dots, in_sem, d1_s, d1_r, x_s, x_r,
+def rest_kernel(n, p_ref, sqs_ref, conv_ref, gain_ref, sel_ref, cot_hbm, w_hbm, taps_ref, gated_ref, proj_ref,
+                act, all_ref, cq, w_buf, d_r, sx, rx, back, ret, mg, pr, ext, halo, dots, in_sem, w_sem, d1_s, d1_r, x_s, x_r,
                 a_s, a_r, o_sem, up_s, up_r, dn_s, dn_r, y_s, y_r, m_s, m_r, b_s, b_r, e_s, e_r, t_s, t_r, h_s, h_r):
     me, q, twin, across = places()
     twin_across = (twin + 2) % 4
@@ -303,12 +303,14 @@
     before = (me + n - 1) % n
     load = pltpu.make_async_copy(cot_hbm.at[:, span(q, cols)], cq, in_sem)
     load.start()
+    w_load = pltpu.make_async_copy(w_hbm, w_buf, w_sem)
+    w_load.start()
     greet([((me + j) % n, q) for j in range(1, n)] + [(me, twin), (me, across), (me, twin_across)])
     order = list(range(n - 1, -1, -1))
     waits = []
     firsts = {}
-    for j in order:
-        for k, quarter in enumerate((twin_across, twin)):
+    for k, quarter in enumerate((twin_across, twin)):
+        for j in order:
             part = span(toggled(me, j), rows)
             c = send(p_ref.at[part, span(quarter, cols)], d_r.at[k, part], d1_s.at[k, j], d1_r.at[k, j], (me, twin))
             c.start()
@@ -384,12 +386,8 @@
     crossing += [first(j) for j in order[2:]]
     for at, j in enumerate(order):
         second(j, crossing[at])
-        if at == 1:
-            take(0)
-            start_ways(1)
-        if at == 4:
-            take(1)
-            start_ways(2)
+    take(0)
+    start_ways(1)
     load.wait()
     for j in order[:-1]:
         got = send(back.at[span(me, rows)], ret.at[span(toggled(me, j), rows)], a_s.at[j], a_r.at[j], (me, q))
@@ -402,7 +400,7 @@
     to_x.start()
     to_twin = send(mine, mine, m_s.at[1], m_r.at[1], (me, twin))
     to_twin.start()
-    take(2)
+    take(1)
     sig = jax.nn.sigmoid(normed)
     slope = sig * (1.0 + normed * (1.0 - sig)) * gain
     theirs = mg.at[:, span(across, cols)]
@@ -422,7 +420,9 @@
         incoming.append(send(mg.at[span(q, share), span(d, block)], pr.at[d, q], b_s.at[j], b_r.at[j], (d, q)))
     kept = pltpu.make_async_copy(mg.at[span(q, share), span(me, block)], pr.at[me, q], o_sem.at[1])
     kept.start()
-    into = lax.dot_general(mg[...], w_ref[...], (((1,), (1,)), ((), ())), preferred_element_type=f32)
+    start_ways(2)
+    w_load.wait()
+    into = lax.dot_general(mg[...], w_buf[...], (((1,), (1,)), ((), ())), preferred_element_type=f32)
     scaled = into * slope
     dots[0] = jnp.broadcast_to(as_row(jnp.sum(conv * scaled, axis=1, keepdims=True)), dots.shape[1:])
     small = []
@@ -452,6 +452,7 @@
     pl.when(me > 0)(shift.start)
     spread[0].wait_recv()
     spread[2].start()
+    take(2)
 
     @pl.when(me < n - 1)
     def _():
@@ -536,12 +537,13 @@
     gated_grad, proj_grad = pl.pallas_call(
         functools.partial(rest_kernel, n),
         out_shape=(shape((tokens_here, quarter), f32), shape((model_width // n, quarter), f32)),
-        in_specs=[VMEM] * 5 + [anywhere] + [VMEM] * 2,
+        in_specs=[VMEM] * 5 + [anywhere] * 2 + [VMEM],
         out_specs=(VMEM, VMEM),
         scratch_shapes=[
             pltpu.VMEM((tokens_here, quarter), bf16),
             pltpu.VMEM((n * tokens_here, quarter), bf16),
             pltpu.VMEM((tokens_here, quarter), bf16),
+            pltpu.VMEM(out_weight.shape, bf16),
             pltpu.VMEM((2, total_rows, quarter), bf16),
         ]
         + [pltpu.VMEM((total_rows, quarter), bf16)] * 4
@@ -551,6 +553,7 @@
             pltpu.VMEM((tokens_here + pad, quarter), f32),
             pltpu.VMEM((2, pad, quarter), bf16),
             pltpu.VMEM((4, 8, tokens_here), f32),
+            DMA,
             DMA,
         ]
         + [DMA((2, n))] * 2

time: 106 us -> 101 us (0.953)
  Pallas kernels: 88.2 us -> 83.8 us
    pallas_call x1, Pallas kernels: 49.1 us -> 44.7 us  [near_plan(): pl.pallas_call(functools.partial(rest_kernel, n), out_shape=(shape((token...]
where the time goes in v3:
time: 101 us
  Pallas kernels  83.8 us (83%)
  matrix products  12.1 us (12%)
  local copies, waits for them, and re-layouts  4.38 us (4%)
    pallas_call x1, Pallas kernels, near_plan(): pl.pallas_call(functools.partial(rest_kernel, n), out_shape=(shape((token...  44.7 us
    pallas_call x1, Pallas kernels, near_plan(): pl.pallas_call(functools.partial(dispatch_kernel, n), out_shape=(shape((2...  39.1 us
    unnamed x10, local copies, waits for them, and re-layouts  4.38 us
    dot_general x1, matrix products, expert_backward(): pre_gate = jnp.dot(x_rows, w_gate, preferred_element_type=jnp.float32)  2.45 us
    dot_general x1, matrix products, expert_backward(): lax.dot_general(up_pre_grad, w_up, (((1,), (1,)), ((), ())), preferred_el...  2.11 us

profile of v3, /device:TPU:0, one launch (start us, length us, event | category | flops | bytes accessed | tf_op | source)
XLA Modules:
  0.0 101.0 jit_solution(11920661040897534601)
XLA Ops:
  0.6 0.0 copy-start
  0.6 0.0 copy-start.1
  0.7 39.1 %dispatch.1 = (bf16[2,512,2048]{2,1,0:T(8,128)(2,1)}, bf16[512,128]{1,0:T(8,128)(2,1)}, f32[4,8,128]{2,1,0:T(8,128)}) custom-call(bf16[128,2048]{1,0:T(8,128)(2,1)} %x_hbm.1, bf16[128,2048]{1,0:T(8,128)(2,1)} %cot_hbm.3, s32[2,128]{1,0:T(2,128)} %bitcast.45, f32[2,128]{1,0:T(2,128)} %bitcast.46, bf16[128,512]{1,0:T(8,128)(2,1)} %conv_ref.3), custom_call_target="tpu_custom_call" | custom-call | tf_op jit(solution)/shard_map/dispatch/pallas_call | solution.py:514
  39.8 0.0 copy-start.2
  39.8 0.0 copy-done
  39.8 2.5 %fusion.8 = f32[512,256]{1,0:T(8,128)S(1)} fusion(bf16[2,512,2048]{2,1,0:T(8,128)(2,1)} %get-tuple-element.10, bf16[1,2048,256]{2,1,0:T(8,128)(2,1)S(1)} %copy-done), kind=kOutput, calls=%fused_computation.12 | convolution fusion | flops 536870912 | bytes 3670016 | tf_op jit(solution)/shard_map/dot_general | solution.py:20
  42.3 0.0 copy-done.1
  42.3 0.3 copy-done.2
  42.6 0.0 copy-start.3
  42.6 0.7 fusion.10
  43.3 0.5 copy-done.3
  43.8 0.8 multiply_convert_fusion.1
  44.7 1.8 %fusion.2 = bf16[1,256,2048]{2,1,0:T(8,128)(2,1)} fusion(bf16[2,512,2048]{2,1,0:T(8,128)(2,1)S(1)} %copy-done.2, f32[512,256]{1,0:T(8,128)S(1)} %fusion.10, f32[512,256]{1,0:T(8,128)S(1)} %fusion.8), kind=kOutput, calls=%fused_computation.6 | convolution fusion | flops 538181632 | bytes 4194304 | tf_op jit(solution)/shard_map/dot_general | solution.py:24
  46.4 1.8 %fusion.1 = bf16[1,2048,256]{2,1,0:T(8,128)(2,1)} fusion(bf16[512,256]{1,0:T(8,128)(2,1)S(1)} %get-tuple-element.15, bf16[2,512,2048]{2,1,0:T(8,128)(2,1)S(1)} %copy-done.2), kind=kOutput, calls=%fused_computation.5 | convolution fusion | flops 537395200 | bytes 3407872 | tf_op jit(solution)/shard_map/dot_general | solution.py:37
  48.2 1.7 %fusion = bf16[1,2048,256]{2,1,0:T(8,128)(2,1)} fusion(bf16[512,256]{1,0:T(8,128)(2,1)S(1)} %get-tuple-element.16, bf16[2,512,2048]{2,1,0:T(8,128)(2,1)S(1)} %copy-done.2), kind=kOutput, calls=%fused_computation.4 | convolution fusion | flops 537395200 | bytes 3407872 | tf_op jit(solution)/shard_map/dot_general | solution.py:34
  49.9 0.7 fusion.18
  50.7 2.1 %add_convert_fusion.p_ref = bf16[512,2048]{1,0:T(8,128)(2,1)} fusion(f32[512,2048]{1,0:T(8,128)S(1)} %fusion.18, bf16[512,256]{1,0:T(8,128)(2,1)S(1)} %get-tuple-element.15, bf16[1,2048,256]{2,1,0:T(8,128)(2,1)S(1)} %copy-done.1), kind=kOutput, calls=%fused_computation | convolution fusion | flops 538968064 | bytes 7602176 | tf_op jit(solution)/shard_map/dot_general | solution.py:43
  52.8 44.7 %rest.1 = (f32[128,512]{1,0:T(8,128)}, f32[256,512]{1,0:T(8,128)}) custom-call(bf16[512,2048]{1,0:T(8,128)(2,1)} %add_convert_fusion.p_ref, f32[4,8,128]{2,1,0:T(8,128)} %get-tuple-element.11.sqs_ref, bf16[128,512]{1,0:T(8,128)(2,1)} %conv_ref.3, f32[1,512]{1,0:T(1,128)} %bitcast.44, bf16[512,128]{1,0:T(8,128)(2,1)} %get-tuple-element.12.sel_ref, ...), custom_call_target="tpu_custom_call" | custom-call | tf_op jit(solution)/shard_map/rest/pallas_call | solution.py:537
  97.5 1.9 %copy.18 = f32[256,512]{1,0:T(8,128)} copy(f32[256,512]{1,0:T(8,128)} %get-tuple-element.25) | data formatting | bytes 1048576
  99.3 1.7 %copy.19 = f32[128,512]{1,0:T(8,128)} copy(f32[128,512]{1,0:T(8,128)} %get-tuple-element.26) | data formatting | bytes 524288
Async XLA Ops:
  0.6 39.2 %copy-start = (bf16[1,2048,256]{2,1,0:T(8,128)(2,1)S(1)}, bf16[1,2048,256]{2,1,0:T(8,128)(2,1)}, u32[]{:S(2)}) copy-start(bf16[1,2048,256]{2,1,0:T(8,128)(2,1)} %param.16) | copy-start | bytes 3145732
  0.6 41.6 %copy-start.1 = (bf16[1,2048,256]{2,1,0:T(8,128)(2,1)S(1)}, bf16[1,2048,256]{2,1,0:T(8,128)(2,1)}, u32[]{:S(2)}) copy-start(bf16[1,2048,256]{2,1,0:T(8,128)(2,1)} %param.17) | copy-start | bytes 3145732
  39.8 2.8 %copy-start.2 = (bf16[2,512,2048]{2,1,0:T(8,128)(2,1)S(1)}, bf16[2,512,2048]{2,1,0:T(8,128)(2,1)}, u32[]{:S(2)}) copy-start(bf16[2,512,2048]{2,1,0:T(8,128)(2,1)} %get-tuple-element.10) | copy-start | bytes 12582916
  42.6 1.2 %copy-start.3 = (bf16[1,256,2048]{2,1,0:T(8,128)(2,1)S(1)}, bf16[1,256,2048]{2,1,0:T(8,128)(2,1)}, u32[]{:S(2)}) copy-start(bf16[1,256,2048]{2,1,0:T(8,128)(2,1)} %param.18) | copy-start | bytes 3145732
